TPU v7x, 512 devices: a whole 4x4x16 slice. The times are simulated.
512 devices in a mesh: row: 64 (over z, y), col: 8 (over x, core).
Axes of the slice: x: 4, y: 4, z: 16, core: 2. Of those that a mesh axis runs over, the one named last changes fastest.
Arguments:
- tokens: bfloat16 [8, 12288, 2048], P('col', 'row'), may hold values from -6 to 6
- proj_in: bfloat16 [2048, 512], P('col'), may hold values from -0.125 to 0.125
- proj_out: bfloat16 [512, 2048], P(None, 'row'), may hold values from -0.25 to 0.25
Outputs:
- output: bfloat16 [8, 12288, 2048], P('col', 'row')
All inputs are finite; a program needn't handle non-finite values.
Results may differ from a plain program's by a relative error of at most 0.0083.
Values may be sent and summed in bfloat16 or wider, within the bound.
A program may use at most 64 MiB of HBM per device.

v0:
```python
import math
import jax
import jax.numpy as jnp
from jax import lax
from jax.sharding import Mesh
from jax.sharding import PartitionSpec as P

GRP = 128
ROW = ("row_0", "row_1")
highest = lax.Precision.HIGHEST
span_inner = 128


def copy_for_each(array, axis):
    copies = jnp.broadcast_to(array, (lax.axis_size(axis), *array.shape))
    return lax.all_to_all(copies, axis, split_axis=0, concat_axis=0, tiled=True)


def joined_along(tiles, dim):
    lengths = list(tiles.shape[1:])
    lengths[dim] *= tiles.shape[0]
    return jnp.moveaxis(tiles, 0, dim).reshape(lengths)


def gathered_copies(array, axis, dim):
    tiles = copy_for_each(array, axis)
    return joined_along(tiles, dim)


def in_blocks(array, dim, count):
    before, after = (array.shape[:dim], array.shape[dim + 1 :])
    return jnp.moveaxis(array.reshape(*before, count, -1, *after), dim, 0)


def turned_blocks(tiles, axes, sequence):
    inside = tiles.shape[1:]
    result = tiles.reshape(*(lax.axis_size(a) for a in axes), *inside)
    for k in sequence:
        result = lax.all_to_all(result, axes[k], k, k, tiled=True)
    return result.reshape(-1, *inside)


def exchange_by_axis(array, axes, sequence, split_dim, concat_dim):
    tiles = in_blocks(array, split_dim, lax.axis_size(axes))
    return joined_along(turned_blocks(tiles, axes, sequence), concat_dim)


def circle(height, breadth, period):
    product = lax.iota(jnp.int32, height)[:, None] * lax.iota(jnp.int32, breadth)[None, :] % period
    angle = product.astype(jnp.float32) * (2.0 * math.pi / period)
    return (jnp.cos(angle), jnp.sin(angle))


def mirror(values):
    return jnp.concatenate([values[:, :1], jnp.flip(values[:, 1:], 1)], 1)


def positions(piece):
    real_in = piece[0, 0]
    imag_in = piece[1, 0]
    count, length = real_in.shape
    outer = length // span_inner
    real_in = real_in.reshape(count, outer, span_inner)
    imag_in = imag_in.reshape(count, outer, span_inner)
    cos_one, sin_one = circle(outer, outer, outer)
    first_re = jnp.einsum("ab,kbq->kaq", cos_one, real_in, precision=highest) - jnp.einsum(
        "ab,kbq->kaq", sin_one, imag_in, precision=highest
    )
    first_im = jnp.einsum("ab,kbq->kaq", sin_one, real_in, precision=highest) + jnp.einsum(
        "ab,kbq->kaq", cos_one, imag_in, precision=highest
    )
    twist_c, twist_s = circle(outer, span_inner, length)
    turned_re = first_re * twist_c - first_im * twist_s
    turned_im = first_re * twist_s + first_im * twist_c
    cos_two, sin_two = circle(span_inner, span_inner, span_inner)
    factor = 1.0 / math.sqrt(GRP * length)
    real_out = jnp.einsum("kaq,qb->kba", turned_re, cos_two, precision=highest) - jnp.einsum(
        "kaq,qb->kba", turned_im, sin_two, precision=highest
    )
    real_out = real_out.reshape(count, length) * factor
    imag_out = jnp.einsum("kaq,qb->kba", turned_re, sin_two, precision=highest) + jnp.einsum(
        "kaq,qb->kba", turned_im, cos_two, precision=highest
    )
    imag_out = imag_out.reshape(count, length) * factor
    return jnp.stack([real_out, imag_out], 1)


def shards(tokens, proj_in, proj_out):
    seq_rows = tokens[0]
    local_len = seq_rows.shape[0]
    features = proj_in.shape[1]
    groups = features // GRP
    mapped = jnp.dot(
        seq_rows, gathered_copies(proj_in, "col", 0), preferred_element_type=jnp.float32
    ).astype(jnp.bfloat16)
    values = mapped.astype(jnp.float32).reshape(local_len, groups, GRP)
    cos_c, sin_c = circle(GRP, GRP, GRP)
    half = GRP // 2
    real_table = cos_c[:, :half]
    imag_table = jnp.concatenate([cos_c[:, half : half + 1], sin_c[:, 1:half]], 1)
    real_part = jnp.einsum("pgc,cs->gsp", values, real_table, precision=highest)
    imag_part = jnp.einsum("pgc,cs->gsp", values, imag_table, precision=highest)
    ways = lax.axis_size(ROW)
    slots = groups * real_table.shape[1]
    per_dev = slots // ways
    stacked = jnp.stack(
        [real_part.reshape(ways, per_dev, local_len), imag_part.reshape(ways, per_dev, local_len)],
        0,
    )
    spectra = positions(
        lax.all_to_all(
            stacked.astype(jnp.bfloat16), ROW, split_axis=1, concat_axis=3, tiled=True
        ).astype(stacked.dtype)
    )
    slot_ids = lax.axis_index(ROW) * per_dev + lax.iota(jnp.int32, per_dev)
    special = (slot_ids % half == 0)[:, None]
    real_g = spectra[:, 0]
    imag_g = spectra[:, 1]
    lower = jnp.where(special, 0.5 * (real_g + mirror(real_g)), real_g)
    upper = jnp.where(special, 0.5 * (imag_g + mirror(imag_g)), mirror(real_g))
    outgoing = jnp.stack([lower, upper], 1).astype(jnp.bfloat16)
    back = exchange_by_axis(outgoing, ROW, (0, 1), 2, 0)
    paired = back.reshape(groups, half, 2, local_len)
    low_half = paired[:, :, 0]
    high_half = paired[:, :, 1]
    mixed = jnp.concatenate([low_half, high_half[:, :1], jnp.flip(high_half[:, 1:], 1)], 1).reshape(
        features, local_len
    )
    result = lax.dot_general(
        mixed,
        lax.all_gather(proj_out, ROW, axis=1, tiled=True),
        (((0,), (0,)), ((), ())),
        preferred_element_type=jnp.float32,
    )
    return result.astype(jnp.bfloat16)[None]


def solution(mesh):
    split = Mesh(mesh.devices.reshape(16, 4, mesh.shape["col"]), ("row_0", "row_1", "col"))
    return jax.shard_map(
        shards,
        mesh=split,
        in_specs=(P("col", ROW, None), P("col", None), P(None, ROW)),
        out_specs=P("col", ROW, None),
        check_vma=False,
    )
```

profile of v0, /device:TPU:2, one launch (start us, length us, event | category | flops | bytes accessed | tf_op | source)
XLA Modules:
  0.0 218.3 jit_solution(16846580736775457972)
XLA Ops:
  6.5 2.5 %broadcast_in_dim.13 = bf16[8,256,512]{2,1,0:T(8,128)(2,1)} broadcast(bf16[256,512]{1,0:T(8,128)(2,1)} %param.4), dimensions={1,2} | broadcast | bytes 2359296 | tf_op jit(solution)/shard_map/broadcast_in_dim | solution.py:15
  9.1 9.4 %all-to-all-start = ((bf16[8,256,512]{2,1,0:T(8,128)(2,1)}), bf16[8,256,512]{2,1,0:T(8,128)(2,1)S(1)}, u32[]{:S(2)}, u32[]{:S(2)}) async-start(bf16[8,256,512]{2,1,0:T(8,128)(2,1)} %broadcast_in_dim.13), calls=%async_computation | async-start | bytes 4194304 | tf_op jit(solution)/shard_map/all_to_all | solution.py:16
  18.5 0.3 fusion.54
  18.7 0.3 fusion.53
  19.0 25.2 %all-to-all-done = bf16[8,256,512]{2,1,0:T(8,128)(2,1)S(1)} async-done(((bf16[8,256,512]{2,1,0:T(8,128)(2,1)}), bf16[8,256,512]{2,1,0:T(8,128)(2,1)S(1)}, u32[]{:S(2)}, u32[]{:S(2)}) %all-to-all-start) | async-done | bytes 2097184 | tf_op jit(solution)/shard_map/all_to_all | solution.py:16
  44.2 0.6 fusion.1
  44.8 0.5 fusion.8
  45.3 0.5 fusion.9
  45.9 0.9 pad_maximum_fusion
  46.8 14.1 %all-to-all-start.1 = ((bf16[2,64,4,192]{3,2,0,1:T(4,128)(2,1)}), bf16[2,64,4,192]{3,2,0,1:T(4,128)(2,1)S(1)}, u32[]{:S(2)}, u32[]{:S(2)}) async-start(bf16[2,64,4,192]{3,2,0,1:T(4,128)(2,1)} %pad_maximum_fusion), calls=%async_computation.1 | async-start | bytes 524288 | tf_op jit(solution)/shard_map/all_to_all | solution.py:111
  61.0 0.7 all-gather.2.cloned.1.call-update
  61.7 0.2 fusion.39
  61.9 21.3 %all-to-all-done.1 = bf16[2,64,4,192]{3,2,0,1:T(4,128)(2,1)S(1)} async-done(((bf16[2,64,4,192]{3,2,0,1:T(4,128)(2,1)}), bf16[2,64,4,192]{3,2,0,1:T(4,128)(2,1)S(1)}, u32[]{:S(2)}, u32[]{:S(2)}) %all-to-all-start.1) | async-done | bytes 196640 | tf_op jit(solution)/shard_map/all_to_all | solution.py:111
  83.4 0.2 reshape_squeeze.6
  83.6 0.4 fusion.35
  84.0 0.4 fusion.31
  84.4 0.2 reshape_squeeze.7
  84.6 0.4 fusion.6
  85.0 0.4 fusion.7
  85.4 0.6 fusion.22
  86.0 0.6 fusion.5
  86.6 0.1 copy.68
  86.7 0.2 mul.299
  87.0 0.2 slice.62
  87.2 0.1 mul.298
  87.3 0.6 fusion.18
  87.8 0.6 fusion.3
  88.4 0.1 copy.73
  88.6 0.2 mul.304
  88.8 0.1 mul.303
  88.9 8.4 %reverse = f32[4,12288]{1,0:T(4,128)S(1)} reverse(f32[4,12288]{1,0:T(4,128)S(1)} %bitcast.99), dimensions={1} | reverse | bytes 393216
  97.3 0.2 slice_bitcast_fusion.5
  97.4 0.2 slice.64
  97.6 8.4 %reverse.1 = f32[4,12288]{1,0:T(4,128)S(1)} reverse(f32[4,12288]{1,0:T(4,128)S(1)} %bitcast.100), dimensions={1} | reverse | bytes 393216
  106.0 0.2 slice_bitcast_fusion.4
  106.1 0.2 pad_maximum_fusion.2
  106.3 0.2 concatenate.40
  106.5 0.2 pad_maximum_fusion.3
  106.6 0.2 concatenate.44
  107.1 0.3 copy.87
  107.3 20.6 %all_to_all.30 = bf16[16,4,4,2,192]{4,3,2,1,0:T(2,128)(2,1)S(1)} all-to-all(bf16[16,4,4,2,192]{4,3,2,1,0:T(2,128)(2,1)S(1)} %bitcast.98), channel_id=1, replica_groups=mesh['row_0'=16,'row_1'=4,'col'=8] {'row_0'}, dimensions={0} | all-to-all | bytes 393216 | tf_op jit(solution)/shard_map/all_to_all | solution.py:39
  128.0 0.2 copy.77
  128.2 9.7 %all_to_all.31 = bf16[16,4,4,2,192]{4,3,2,0,1:T(2,128)(2,1)S(1)} all-to-all(bf16[16,4,4,2,192]{4,3,2,0,1:T(2,128)(2,1)S(1)} %copy.77), channel_id=1, replica_groups=mesh['row_0'=16,'row_1'=4,'col'=8] {'row_1'}, dimensions={1} | all-to-all | bytes 393216 | tf_op jit(solution)/shard_map/all_to_all | solution.py:39
  137.8 0.2 copy.78
  138.1 0.4 fusion.102
  138.5 0.2 rev.14
  138.8 69.3 %all-gather.2.cloned.1.call-done = bf16[512,2048]{0,1:T(8,128)(2,1)} async-done(((bf16[512,32]{0,1:T(8,128)(2,1)}), bf16[512,2048]{0,1:T(8,128)(2,1)}) %all-gather.2.cloned.1.call-update) | async-done | bytes 2097168 | tf_op jit(solution)/shard_map/all_gather | solution.py:131
  208.1 3.3 %fusion = bf16[1,192,2048]{2,1,0:T(8,128)(2,1)} fusion(bf16[512,192]{1,0:T(8,128)(2,1)S(1)} %bitcast.96, bf16[512,2048]{0,1:T(8,128)(2,1)} %all-gather.2.cloned.1.call-done), kind=kOutput, calls=%fused_computation.1 | convolution fusion | flops 403046400 | bytes 3080192 | tf_op jit(solution)/shard_map/dot_general | solution.py:129
  (21 shorter events, 0.7 us)
Async XLA Ops:
  6.5 37.7 %copy-start = (bf16[1,192,2048]{2,1,0:T(8,128)(2,1)S(1)}, bf16[1,192,2048]{2,1,0:T(8,128)(2,1)}, u32[]{:S(2)}) copy-start(bf16[1,192,2048]{2,1,0:T(8,128)(2,1)} %param.3) | copy-start | bytes 2359300
  9.1 35.1 %all-to-all-start = ((bf16[8,256,512]{2,1,0:T(8,128)(2,1)}), bf16[8,256,512]{2,1,0:T(8,128)(2,1)S(1)}, u32[]{:S(2)}, u32[]{:S(2)}) async-start(bf16[8,256,512]{2,1,0:T(8,128)(2,1)} %broadcast_in_dim.13), calls=%async_computation | async-start | bytes 4194304 | tf_op jit(solution)/shard_map/all_to_all | solution.py:16
  46.8 36.5 %all-to-all-start.1 = ((bf16[2,64,4,192]{3,2,0,1:T(4,128)(2,1)}), bf16[2,64,4,192]{3,2,0,1:T(4,128)(2,1)S(1)}, u32[]{:S(2)}, u32[]{:S(2)}) async-start(bf16[2,64,4,192]{3,2,0,1:T(4,128)(2,1)} %pad_maximum_fusion), calls=%async_computation.1 | async-start | bytes 524288 | tf_op jit(solution)/shard_map/all_to_all | solution.py:111
  60.9 147.2 %all-gather.2.cloned.1.call-start = ((), (), s32[]{:S(2)}) async-start(), calls=%async_computation.4 | async-start | bytes 2129920 | tf_op jit(solution)/shard_map/all_gather | solution.py:131
Sparse Core Ops, SparseCore 0:
  64.7 143.3 all-gather.1
where the time goes:
time: 219 us; the launch traced here: 218 us
  waiting for transfers between devices  116 us (53%)
  blocking collectives  30.3 us (14%)
  starting transfers between devices  23.6 us (11%)
  local copies, waits for them, and re-layouts  23.1 us (11%)
  between operations  13.7 us (6%)
  matrix products  8.83 us (4%)
  other arithmetic  2.26 us (1%)
    all_gather x1, waiting for transfers between devices, shards(): lax.all_gather(proj_out, ROW, axis=1, tiled=True)  69.3 us
    all_to_all x2, blocking collectives, turned_blocks(): result = lax.all_to_all(result, axes[k], k, k, tiled=True)  30.3 us
    all_to_all x1, waiting for transfers between devices, copy_for_each(): return lax.all_to_all(copies, axis, split_axis=0, concat_axis=0, tiled=True)  25.2 us
    all_to_all x1, waiting for transfers between devices, shards(): lax.all_to_all(stacked.astype(jnp.bfloat16), ROW, split_axis=1, concat_ax...  21.3 us
    unnamed x6, local copies, waits for them, and re-layouts  16.8 us
    all_to_all x1, starting transfers between devices, shards(): lax.all_to_all(stacked.astype(jnp.bfloat16), ROW, split_axis=1, concat_ax...  14.1 us
    all_to_all x1, starting transfers between devices, copy_for_each(): return lax.all_to_all(copies, axis, split_axis=0, concat_axis=0, tiled=True)  9.39 us
  transfers between devices with their start and end apart: 3, of which 3 were waited for; matrix products, arithmetic and copies ran while one was open for 12% of the time, Pallas kernels for 0%

commit v1 on v0

--- a/solution.py
+++ b/solution.py
@@ -9,6 +9,11 @@
 ROW = ("row_0", "row_1")
 highest = lax.Precision.HIGHEST
 span_inner = 128
+
+
+def gather_over(x, mesh_axis, dim):
+    sent = jnp.stack([x] * lax.axis_size(mesh_axis))
+    return jnp.concatenate(lax.all_to_all(sent, mesh_axis, 0, 0), axis=dim)
 
 
 def copy_for_each(array, axis):
@@ -128,7 +133,7 @@
     )
     result = lax.dot_general(
         mixed,
-        lax.all_gather(proj_out, ROW, axis=1, tiled=True),
+        gather_over(proj_out, ROW, 1),
         (((0,), (0,)), ((), ())),
         preferred_element_type=jnp.float32,
     )

time: 219 us -> 240 us (1.096)
  the two profiles are of different devices: /device:TPU:2 before, /device:TPU:8 now
where the time goes in v1:
time: 240 us
  waiting for transfers between devices  144 us (60%)
  starting transfers between devices  31 us (13%)
  blocking collectives  30 us (12%)
  local copies, waits for them, and re-layouts  24.7 us (10%)
  matrix products  7.24 us (3%)
    all_to_all x1, waiting for transfers between devices, gather_over(): return jnp.concatenate(lax.all_to_all(sent, mesh_axis, 0, 0), axis=dim)  96.6 us
    all_to_all x2, blocking collectives, turned_blocks(): result = lax.all_to_all(result, axes[k], k, k, tiled=True)  30 us
    all_to_all x1, waiting for transfers between devices, copy_for_each(): return lax.all_to_all(copies, axis, split_axis=0, concat_axis=0, tiled=True)  26.6 us
    all_to_all x1, waiting for transfers between devices, shards(): lax.all_to_all(stacked.astype(jnp.bfloat16), ROW, split_axis=1, concat_ax...  21 us
    all_to_all x1, starting transfers between devices, shards(): lax.all_to_all(stacked.astype(jnp.bfloat16), ROW, split_axis=1, concat_ax...  18.7 us
    unnamed x8, local copies, waits for them, and re-layouts  16.8 us
    all_to_all x1, starting transfers between devices, gather_over(): return jnp.concatenate(lax.all_to_all(sent, mesh_axis, 0, 0), axis=dim)  7.93 us
  transfers between devices with their start and end apart: 3, of which 3 were waited for; matrix products, arithmetic and copies ran while one was open for 1% of the time, Pallas kernels for 0%

profile of v1, /device:TPU:8, one launch (start us, length us, event | category | flops | bytes accessed | tf_op | source)
XLA Modules:
  0.0 239.7 jit_solution(14200561163914746593)
XLA Ops:
  0.0 2.5 %broadcast_in_dim.13 = bf16[8,256,512]{2,1,0:T(8,128)(2,1)} broadcast(bf16[256,512]{1,0:T(8,128)(2,1)} %param.4), dimensions={1,2} | broadcast | bytes 2359296 | tf_op jit(solution)/shard_map/broadcast_in_dim | solution.py:20
  2.5 4.3 %all-to-all-start = ((bf16[8,256,512]{2,1,0:T(8,128)(2,1)}), bf16[8,256,512]{2,1,0:T(8,128)(2,1)S(1)}, u32[]{:S(2)}, u32[]{:S(2)}) async-start(bf16[8,256,512]{2,1,0:T(8,128)(2,1)} %broadcast_in_dim.13), calls=%async_computation | async-start | bytes 4194304 | tf_op jit(solution)/shard_map/all_to_all | solution.py:21
  6.8 0.3 fusion.54
  7.1 0.3 fusion.53
  7.4 26.6 %all-to-all-done = bf16[8,256,512]{2,1,0:T(8,128)(2,1)S(1)} async-done(((bf16[8,256,512]{2,1,0:T(8,128)(2,1)}), bf16[8,256,512]{2,1,0:T(8,128)(2,1)S(1)}, u32[]{:S(2)}, u32[]{:S(2)}) %all-to-all-start) | async-done | bytes 2097184 | tf_op jit(solution)/shard_map/all_to_all | solution.py:21
  34.0 0.6 fusion.1
  34.6 0.5 fusion.8
  35.1 0.5 fusion.9
  35.7 0.9 pad_maximum_fusion
  36.6 18.7 %all-to-all-start.1 = ((bf16[2,64,4,192]{3,2,0,1:T(4,128)(2,1)}), bf16[2,64,4,192]{3,2,0,1:T(4,128)(2,1)S(1)}, u32[]{:S(2)}, u32[]{:S(2)}) async-start(bf16[2,64,4,192]{3,2,0,1:T(4,128)(2,1)} %pad_maximum_fusion), calls=%async_computation.1 | async-start | bytes 524288 | tf_op jit(solution)/shard_map/all_to_all | solution.py:116
  55.4 0.2 fusion.39
  55.6 21.0 %all-to-all-done.1 = bf16[2,64,4,192]{3,2,0,1:T(4,128)(2,1)S(1)} async-done(((bf16[2,64,4,192]{3,2,0,1:T(4,128)(2,1)}), bf16[2,64,4,192]{3,2,0,1:T(4,128)(2,1)S(1)}, u32[]{:S(2)}, u32[]{:S(2)}) %all-to-all-start.1) | async-done | bytes 196640 | tf_op jit(solution)/shard_map/all_to_all | solution.py:116
  76.7 0.2 reshape_squeeze.6
  76.9 0.4 fusion.31
  77.3 0.4 fusion.35
  77.7 0.2 reshape_squeeze.7
  77.9 0.4 fusion.7
  78.3 0.4 fusion.6
  78.8 0.6 fusion.18
  79.3 0.6 fusion.3
  79.9 0.1 copy.74
  80.1 0.2 mul.304
  80.4 0.2 slice.64
  80.6 0.6 fusion.22
  81.2 0.6 fusion.5
  81.8 0.1 copy.69
  81.9 0.2 mul.299
  82.1 0.1 mul.298
  82.2 0.2 slice.62
  82.4 8.4 %reverse.1 = f32[4,12288]{1,0:T(4,128)S(1)} reverse(f32[4,12288]{1,0:T(4,128)S(1)} %bitcast.103), dimensions={1} | reverse | bytes 393216
  90.8 0.2 slice_bitcast_fusion.4
  90.9 0.2 pad_maximum_fusion.3
  91.1 0.2 concatenate.44
  91.3 8.4 %reverse = f32[4,12288]{1,0:T(4,128)S(1)} reverse(f32[4,12288]{1,0:T(4,128)S(1)} %bitcast.104), dimensions={1} | reverse | bytes 393216
  99.6 0.2 slice_bitcast_fusion.5
  99.8 0.2 pad_maximum_fusion.2
  100.0 0.2 concatenate.40
  100.4 0.3 copy.88
  100.7 20.3 %all_to_all.35 = bf16[16,4,4,2,192]{4,3,2,1,0:T(2,128)(2,1)S(1)} all-to-all(bf16[16,4,4,2,192]{4,3,2,1,0:T(2,128)(2,1)S(1)} %bitcast.102), channel_id=1, replica_groups=mesh['row_0'=16,'row_1'=4,'col'=8] {'row_0'}, dimensions={0} | all-to-all | bytes 393216 | tf_op jit(solution)/shard_map/all_to_all | solution.py:44
  121.0 0.2 copy.78
  121.2 9.7 %all_to_all.36 = bf16[16,4,4,2,192]{4,3,2,0,1:T(2,128)(2,1)S(1)} all-to-all(bf16[16,4,4,2,192]{4,3,2,0,1:T(2,128)(2,1)S(1)} %copy.78), channel_id=1, replica_groups=mesh['row_0'=16,'row_1'=4,'col'=8] {'row_1'}, dimensions={1} | all-to-all | bytes 393216 | tf_op jit(solution)/shard_map/all_to_all | solution.py:44
  130.9 1.6 stack.9
  132.5 7.9 %all-to-all-start.4 = ((bf16[64,512,32]{1,2,0:T(8,128)(2,1)}), bf16[64,512,32]{1,2,0:T(8,128)(2,1)S(1)}, u32[]{:S(2)}, u32[]{:S(2)}) async-start(bf16[64,512,32]{1,2,0:T(8,128)(2,1)} %stack.9), calls=%async_computation.4 | async-start | bytes 4194304 | tf_op jit(solution)/shard_map/all_to_all | solution.py:16
  140.4 0.2 copy.79
  140.6 0.4 fusion.102
  141.1 0.2 rev.14
  141.4 96.6 %all-to-all-done.4 = bf16[64,512,32]{1,2,0:T(8,128)(2,1)S(1)} async-done(((bf16[64,512,32]{1,2,0:T(8,128)(2,1)}), bf16[64,512,32]{1,2,0:T(8,128)(2,1)S(1)}, u32[]{:S(2)}, u32[]{:S(2)}) %all-to-all-start.4) | async-done | bytes 2097184 | tf_op jit(solution)/shard_map/all_to_all | solution.py:16
  238.0 1.7 fusion
  (23 shorter events, 0.7 us)
Async XLA Ops:
  0.0 34.0 %copy-start = (bf16[1,192,2048]{2,1,0:T(8,128)(2,1)S(1)}, bf16[1,192,2048]{2,1,0:T(8,128)(2,1)}, u32[]{:S(2)}) copy-start(bf16[1,192,2048]{2,1,0:T(8,128)(2,1)} %param.3) | copy-start | bytes 2359300
  2.5 31.5 %all-to-all-start = ((bf16[8,256,512]{2,1,0:T(8,128)(2,1)}), bf16[8,256,512]{2,1,0:T(8,128)(2,1)S(1)}, u32[]{:S(2)}, u32[]{:S(2)}) async-start(bf16[8,256,512]{2,1,0:T(8,128)(2,1)} %broadcast_in_dim.13), calls=%async_computation | async-start | bytes 4194304 | tf_op jit(solution)/shard_map/all_to_all | solution.py:21
  36.6 40.0 %all-to-all-start.1 = ((bf16[2,64,4,192]{3,2,0,1:T(4,128)(2,1)}), bf16[2,64,4,192]{3,2,0,1:T(4,128)(2,1)S(1)}, u32[]{:S(2)}, u32[]{:S(2)}) async-start(bf16[2,64,4,192]{3,2,0,1:T(4,128)(2,1)} %pad_maximum_fusion), calls=%async_computation.1 | async-start | bytes 524288 | tf_op jit(solution)/shard_map/all_to_all | solution.py:116
  100.1 30.7 %copy-start.1 = (bf16[512,32]{0,1:T(8,128)(2,1)S(1)}, bf16[512,32]{0,1:T(8,128)(2,1)}, u32[]{:S(2)}) copy-start(bf16[512,32]{0,1:T(8,128)(2,1)} %param.5) | copy-start | bytes 98308
  132.5 105.5 %all-to-all-start.4 = ((bf16[64,512,32]{1,2,0:T(8,128)(2,1)}), bf16[64,512,32]{1,2,0:T(8,128)(2,1)S(1)}, u32[]{:S(2)}, u32[]{:S(2)}) async-start(bf16[64,512,32]{1,2,0:T(8,128)(2,1)} %stack.9), calls=%async_computation.4 | async-start | bytes 4194304 | tf_op jit(solution)/shard_map/all_to_all | solution.py:16
